TPU v7x, 32 devices: a whole 2x2x4 slice. The times are simulated.
32 devices in a mesh: fs: 16 (over z, y, x), tp: 2 (over core).
Axes of the slice: x: 2, y: 2, z: 4, core: 2. Of those that a mesh axis runs over, the one named last changes fastest.
Arguments:
- saved_inputs: bfloat16 [12288, 2048], P('fs'), may hold values from -8 to 8
- input_cot: bfloat16 [12288, 2048], P('fs', 'tp'), may hold values from -0.0546875 to 0.0546875
- gate_cot: bfloat16 [12288, 2048], P('fs', 'tp'), may hold values from -0.0546875 to 0.0546875
- input_master: float32 [2048, 2048], P('fs', 'tp'), may hold values from -6 to 6
- gate_master: float32 [2048, 2048], P('fs', 'tp'), may hold values from -6 to 6
- input_factor: bfloat16 [2048, 256], P('fs'), may hold values from -2 to 2
- gate_factor: bfloat16 [2048, 256], P('fs'), may hold values from -2 to 2
- input_first: float32 [256, 2048], P('fs', 'tp'), may hold values from -6 to 6
- input_second: float32 [256, 2048], P('fs', 'tp'), may hold values from 0.2 to 17
- gate_first: float32 [256, 2048], P('fs', 'tp'), may hold values from -6 to 6
- gate_second: float32 [256, 2048], P('fs', 'tp'), may hold values from 0.2 to 17
Outputs:
- input_step: float32 [2048, 2048], P('fs', 'tp')
- gate_step: float32 [2048, 2048], P('fs', 'tp')
- input_first_new: float32 [256, 2048], P('fs', 'tp')
- input_second_new: float32 [256, 2048], P('fs', 'tp')
- gate_first_new: float32 [256, 2048], P('fs', 'tp')
- gate_second_new: float32 [256, 2048], P('fs', 'tp')
- input_copy: bfloat16 [2048, 2048], P(None, 'tp')
- gate_copy: bfloat16 [2048, 2048], P(None, 'tp')
All inputs are finite; a program needn't handle non-finite values.
Results may differ from a plain program's by a relative error of at most 0.0004.
Values may be sent and summed in bfloat16 or wider, within the bound.
A program may use at most 64 MiB of HBM per device.

v0:
```python
import jax
import jax.numpy as jnp
from jax import lax
from jax.sharding import PartitionSpec as P

D = 2048
W = 2048
first_decay = 0.9
second_decay = 0.9
ratio_floor = 1e-08
mean_floor = 1e-06
step_size = 0.05


def moments(low_rank, first, second):
    first_new = first_decay * first + (1.0 - first_decay) * low_rank
    second_new = second_decay * second + (1.0 - second_decay) * low_rank * low_rank
    ratio = first_new / (jnp.sqrt(second_new) + ratio_floor)
    return (first_new, second_new, ratio)


def local(
    saved_inputs,
    input_cot,
    gate_cot,
    input_master,
    gate_master,
    input_factor,
    gate_factor,
    input_first,
    input_second,
    gate_first,
    gate_second,
):
    col_width = input_cot.shape[1]
    contract = (((0,), (0,)), ((), ()))
    factor_in = input_factor.astype(jnp.float32)
    factor_gate = gate_factor.astype(jnp.float32)
    whole_in, whole_gate = (
        lax.all_gather(input_factor, "fs", axis=0, tiled=True),
        lax.all_gather(gate_factor, "fs", axis=0, tiled=True),
    )
    partial_in = lax.dot_general(
        saved_inputs, input_cot, contract, preferred_element_type=jnp.float32
    )
    partial_gate = lax.dot_general(
        saved_inputs, gate_cot, contract, preferred_element_type=jnp.float32
    )
    cols_in = whole_in.astype(jnp.float32)
    cols_gate = whole_gate.astype(jnp.float32)
    term_in = lax.dot_general(cols_in, partial_in, contract, precision=lax.Precision.HIGHEST)
    term_gate = lax.dot_general(cols_gate, partial_gate, contract, precision=lax.Precision.HIGHEST)
    summed = lax.psum_scatter(
        jnp.concatenate([term_in, term_gate], axis=1), "fs", scatter_dimension=0, tiled=True
    )
    low_in = summed[:, :col_width]
    low_gate = summed[:, col_width:]
    first_in, second_in, ratio_in = moments(low_in, input_first, input_second)
    first_gate, second_gate, ratio_gate = moments(low_gate, gate_first, gate_second)
    piece_in = lax.all_gather(ratio_in, "fs", axis=0, tiled=True)
    piece_gate = lax.all_gather(ratio_gate, "fs", axis=0, tiled=True)
    cols_in = factor_in
    cols_gate = factor_gate
    dir_in = jnp.dot(cols_in, piece_in, precision=lax.Precision.HIGHEST)
    dir_gate = jnp.dot(cols_gate, piece_gate, precision=lax.Precision.HIGHEST)
    square_in, square_gate = lax.psum(
        (jnp.sum(dir_in * dir_in), jnp.sum(dir_gate * dir_gate)), ("fs", "tp")
    )
    step_in = dir_in * lax.rsqrt(square_in / (D * W) + mean_floor)
    step_gate = dir_gate * lax.rsqrt(square_gate / (D * W) + mean_floor)
    local_in = (input_master - step_size * step_in).astype(jnp.bfloat16)
    local_gate = (gate_master - step_size * step_gate).astype(jnp.bfloat16)
    copy_in, copy_gate = (
        lax.all_gather(local_in, "fs", axis=0, tiled=True),
        lax.all_gather(local_gate, "fs", axis=0, tiled=True),
    )
    return (step_in, step_gate, first_in, second_in, first_gate, second_gate, copy_in, copy_gate)


def solution(mesh):
    return jax.shard_map(
        local,
        mesh=mesh,
        in_specs=(
            P("fs", None),
            P("fs", "tp"),
            P("fs", "tp"),
            P("fs", "tp"),
            P("fs", "tp"),
            P("fs", None),
            P("fs", None),
            P("fs", "tp"),
            P("fs", "tp"),
            P("fs", "tp"),
            P("fs", "tp"),
        ),
        out_specs=(
            P("fs", "tp"),
            P("fs", "tp"),
            P("fs", "tp"),
            P("fs", "tp"),
            P("fs", "tp"),
            P("fs", "tp"),
            P(None, "tp"),
            P(None, "tp"),
        ),
        check_vma=False,
    )
```

profile of v0, /device:TPU:0, one launch (start us, length us, event | category | flops | bytes accessed | tf_op | source)
XLA Modules:
  0.0 569.3 jit_solution(10387800890137530023)
XLA Ops:
  9.1 7.2 %fusion.4 = f32[2048,1024]{1,0:T(8,128)} fusion(bf16[768,2048]{1,0:T(8,128)(2,1)S(1)} %copy-done, bf16[768,1024]{1,0:T(8,128)(2,1)} %param.12), kind=kOutput, calls=%fused_computation.17 | convolution fusion | flops 3221225472 | bytes 13107200 | tf_op jit(solution)/shard_map/dot_general | solution.py:43
  16.2 5.7 %fusion.5 = f32[2048,1024]{1,0:T(8,128)} fusion(bf16[768,2048]{1,0:T(8,128)(2,1)S(1)} %copy-done, bf16[768,1024]{1,0:T(8,128)(2,1)S(1)} %copy-done.8), kind=kOutput, calls=%fused_computation.18 | convolution fusion | flops 3221225472 | bytes 13107200 | tf_op jit(solution)/shard_map/dot_general | solution.py:46
  21.9 46.7 %all-gather.7.cloned.1.call-done = bf16[2048,256]{1,0:T(8,128)(2,1)} async-done(((bf16[128,256]{1,0:T(8,128)(2,1)}), bf16[2048,256]{1,0:T(8,128)(2,1)}) %all-gather.7.cloned.1.call-update) | async-done | bytes 1048592 | tf_op jit(solution)/shard_map/all_gather | solution.py:40
  68.6 11.2 %convolution_bitcast_fusion.1 = f32[256,1024]{0,1:T(8,128)} fusion(f32[2048,1024]{1,0:T(8,128)} %fusion.4, bf16[2048,256]{1,0:T(8,128)(2,1)} %all-gather.7.cloned.1.call-done), kind=kOutput, calls=%fused_computation.2 | convolution fusion | flops 6442450944 | bytes 10485760 | tf_op jit(solution)/shard_map/dot_general | solution.py:51
  79.8 45.5 %all-gather.9.cloned.1.call-done = bf16[2048,256]{1,0:T(8,128)(2,1)} async-done(((bf16[128,256]{1,0:T(8,128)(2,1)}), bf16[2048,256]{1,0:T(8,128)(2,1)}) %all-gather.9.cloned.1.call-update) | async-done | bytes 1048592 | tf_op jit(solution)/shard_map/all_gather | solution.py:41
  125.3 9.5 %convolution_bitcast_fusion = f32[256,1024]{0,1:T(8,128)S(1)} fusion(f32[2048,1024]{1,0:T(8,128)} %fusion.5, bf16[2048,256]{1,0:T(8,128)(2,1)} %all-gather.9.cloned.1.call-done), kind=kOutput, calls=%fused_computation.1 | convolution fusion | flops 6442450944 | bytes 10485760 | tf_op jit(solution)/shard_map/dot_general | solution.py:52
  136.3 2.9 copy.65
  139.3 80.6 %reduce-scatter.4.cloned.1.call-done = f32[16,2048]{1,0:T(8,128)} async-done(((f32[256,2048]{1,0:T(8,128)}), f32[16,2048]{1,0:T(8,128)}) %reduce-scatter.4.cloned.1.call-update) | async-done | bytes 131088 | tf_op jit(solution)/shard_map/reduce_scatter | solution.py:53
  219.9 1.6 add_divide_fusion
  222.2 2.0 copy.59
  224.2 50.4 %all-gather.13.cloned.1.call-done = f32[256,1024]{1,0:T(8,128)} async-done(((f32[16,1024]{1,0:T(8,128)}), f32[256,1024]{1,0:T(8,128)}) %all-gather.13.cloned.1.call-update) | async-done | bytes 1048592 | tf_op jit(solution)/shard_map/all_gather | solution.py:61
  274.6 3.7 multiply_reduce_fusion
  278.3 53.4 %all-gather.11.cloned.1.call-done = f32[256,1024]{1,0:T(8,128)} async-done(((f32[16,1024]{1,0:T(8,128)}), f32[256,1024]{1,0:T(8,128)}) %all-gather.11.cloned.1.call-update) | async-done | bytes 1048592 | tf_op jit(solution)/shard_map/all_gather | solution.py:60
  331.7 3.6 multiply_reduce_fusion.1
  335.4 38.6 %all-reduce = (f32[]{:T(128)}, f32[]{:T(128)}) all-reduce(f32[]{:T(128)} %get-tuple-element.47, f32[]{:T(128)} %get-tuple-element.49), channel_id=1, replica_groups=mesh['fs'=16,'tp'=2] {'fs','tp'}, use_global_device_ids=true, to_apply=%region_2.0 | all-reduce | flops 2 | bytes 16 | tf_op jit(solution)/shard_map/psum | solution.py:66
  374.7 2.2 subtract_convert_fusion.1
  376.9 2.0 copy.60
  379.7 2.2 subtract_convert_fusion
  381.9 2.0 copy.61
  383.9 2.0 copy.62
  385.9 80.5 %all-gather.15.cloned.1.call-done = bf16[2048,1024]{0,1:T(8,128)(2,1)} async-done(((bf16[128,1024]{0,1:T(8,128)(2,1)}), bf16[2048,1024]{0,1:T(8,128)(2,1)}) %all-gather.15.cloned.1.call-update) | async-done | bytes 4194320 | tf_op jit(solution)/shard_map/all_gather | solution.py:74
  466.4 6.4 %copy.63 = bf16[2048,1024]{1,0:T(8,128)(2,1)} copy(bf16[2048,1024]{0,1:T(8,128)(2,1)} %all-gather.15.cloned.1.call-done) | data formatting | bytes 8388608
  472.8 83.2 %all-gather.17.cloned.1.call-done = bf16[2048,1024]{0,1:T(8,128)(2,1)} async-done(((bf16[128,1024]{0,1:T(8,128)(2,1)}), bf16[2048,1024]{0,1:T(8,128)(2,1)}) %all-gather.17.cloned.1.call-update) | async-done | bytes 4194320 | tf_op jit(solution)/shard_map/all_gather | solution.py:75
  556.0 6.4 %copy.64 = bf16[2048,1024]{1,0:T(8,128)(2,1)} copy(bf16[2048,1024]{0,1:T(8,128)(2,1)} %all-gather.17.cloned.1.call-done) | data formatting | bytes 8388608
  (33 shorter events, 4.1 us)
Async XLA Ops:
  7.2 1.9 copy-start
  7.2 61.4 %all-gather.7.cloned.1.call-start = ((), (), s32[]{:S(2)}) async-start(), calls=%async_computation.1 | async-start | bytes 1114112 | tf_op jit(solution)/shard_map/all_gather | solution.py:40
  7.9 117.4 %all-gather.9.cloned.1.call-start = ((), (), s32[]{:S(2)}) async-start(), calls=%async_computation.2 | async-start | bytes 1114112 | tf_op jit(solution)/shard_map/all_gather | solution.py:41
  8.7 211.2 %reduce-scatter.4.cloned.1.call-start = ((), (), s32[]{:S(2)}) async-start(), calls=%async_computation.7 | async-start | bytes 2228224 | tf_op jit(solution)/shard_map/reduce_scatter | solution.py:53
  9.1 7.2 %copy-start.8 = (bf16[768,1024]{1,0:T(8,128)(2,1)S(1)}, bf16[768,1024]{1,0:T(8,128)(2,1)}, u32[]{:S(2)}) copy-start(bf16[768,1024]{1,0:T(8,128)(2,1)} %param.13) | copy-start | bytes 4718596
  125.3 9.5 %copy-start.1 = (f32[256,1024]{0,1:T(8,128)S(1)}, f32[256,1024]{0,1:T(8,128)}, u32[]{:S(2)}) copy-start(f32[256,1024]{0,1:T(8,128)} %convolution_bitcast_fusion.1) | copy-start | bytes 3145732
  136.2 83.6 %copy-start.4 = (f32[16,1024]{1,0:T(8,128)S(1)}, f32[16,1024]{1,0:T(8,128)}, u32[]{:S(2)}) copy-start(f32[16,1024]{1,0:T(8,128)} %param.21) | copy-start | bytes 196612
  136.2 83.6 %copy-start.5 = (f32[16,1024]{1,0:T(8,128)S(1)}, f32[16,1024]{1,0:T(8,128)}, u32[]{:S(2)}) copy-start(f32[16,1024]{1,0:T(8,128)} %param.20) | copy-start | bytes 196612
  136.2 83.6 %copy-start.6 = (f32[16,1024]{1,0:T(8,128)S(1)}, f32[16,1024]{1,0:T(8,128)}, u32[]{:S(2)}) copy-start(f32[16,1024]{1,0:T(8,128)} %param.19) | copy-start | bytes 196612
  136.2 83.6 %copy-start.7 = (f32[16,1024]{1,0:T(8,128)S(1)}, f32[16,1024]{1,0:T(8,128)}, u32[]{:S(2)}) copy-start(f32[16,1024]{1,0:T(8,128)} %param.18) | copy-start | bytes 196612
  136.2 138.3 %copy-start.2 = (bf16[128,256]{1,0:T(8,128)(2,1)S(1)}, bf16[128,256]{1,0:T(8,128)(2,1)}, u32[]{:S(2)}) copy-start(bf16[128,256]{1,0:T(8,128)(2,1)} %param.17) | copy-start | bytes 196612
  139.2 192.5 %copy-start.3 = (bf16[128,256]{1,0:T(8,128)(2,1)S(1)}, bf16[128,256]{1,0:T(8,128)(2,1)}, u32[]{:S(2)}) copy-start(bf16[128,256]{1,0:T(8,128)(2,1)} %param.16) | copy-start | bytes 196612
  139.2 135.4 %all-gather.13.cloned.1.call-start = ((), (), s32[]{:S(2)}) async-start(), calls=%async_computation.4 | async-start | bytes 1114112 | tf_op jit(solution)/shard_map/all_gather | solution.py:61
  221.5 110.2 %all-gather.11.cloned.1.call-start = ((), (), s32[]{:S(2)}) async-start(), calls=%async_computation.3 | async-start | bytes 1114112 | tf_op jit(solution)/shard_map/all_gather | solution.py:60
  222.1 244.3 %all-gather.15.cloned.1.call-start = ((), (), s32[]{:S(2)}) async-start(), calls=%async_computation.5 | async-start | bytes 4456448 | tf_op jit(solution)/shard_map/all_gather | solution.py:74
  376.9 179.2 %all-gather.17.cloned.1.call-start = ((), (), s32[]{:S(2)}) async-start(), calls=%async_computation.6 | async-start | bytes 4456448 | tf_op jit(solution)/shard_map/all_gather | solution.py:75
Sparse Core Ops, SparseCore 0:
  10.7 57.7 all-gather.6
  71.3 53.9 all-gather.8
  139.3 80.4 reduce-scatter.3
  223.0 51.4 all-gather.12
  277.8 53.9 all-gather.10
  377.0 89.3 all-gather.14
  469.1 86.8 all-gather.16
where the time goes:
time: 570 us; the launch traced here: 569 us
  waiting for transfers between devices  442 us (78%)
  matrix products  40.9 us (7%)
  blocking collectives  38.6 us (7%)
  local copies, waits for them, and re-layouts  24.2 us (4%)
  between operations  15.6 us (3%)
  other arithmetic  7.42 us (1%)
    all_gather x1, waiting for transfers between devices, local(): lax.all_gather(local_gate, 'fs', axis=0, tiled=True)  83.2 us
    reduce_scatter x1, waiting for transfers between devices, local(): lax.psum_scatter(jnp.concatenate([term_in, term_gate], axis=1), 'fs', sca...  80.6 us
    all_gather x1, waiting for transfers between devices, local(): lax.all_gather(local_in, 'fs', axis=0, tiled=True)  80.5 us
    all_gather x1, waiting for transfers between devices, local(): piece_in = lax.all_gather(ratio_in, 'fs', axis=0, tiled=True)  53.4 us
    all_gather x1, waiting for transfers between devices, local(): piece_gate = lax.all_gather(ratio_gate, 'fs', axis=0, tiled=True)  50.4 us
    all_gather x1, waiting for transfers between devices, local(): lax.all_gather(input_factor, 'fs', axis=0, tiled=True)  46.7 us
    all_gather x1, waiting for transfers between devices, local(): lax.all_gather(gate_factor, 'fs', axis=0, tiled=True)  45.5 us
    psum x1, blocking collectives, local(): lax.psum((jnp.sum(dir_in * dir_in), jnp.sum(dir_gate * dir_gate)), ('fs',...  38.6 us
  transfers between devices with their start and end apart: 7, of which 7 were waited for; matrix products, arithmetic and copies ran while one was open for 8% of the time, Pallas kernels for 0%

commit v1 on v0

--- a/solution.py
+++ b/solution.py
@@ -57,8 +57,11 @@
     low_gate = summed[:, col_width:]
     first_in, second_in, ratio_in = moments(low_in, input_first, input_second)
     first_gate, second_gate, ratio_gate = moments(low_gate, gate_first, gate_second)
-    piece_in = lax.all_gather(ratio_in, "fs", axis=0, tiled=True)
-    piece_gate = lax.all_gather(ratio_gate, "fs", axis=0, tiled=True)
+    piece_in, piece_gate = jnp.split(
+        lax.all_gather(jnp.concatenate([ratio_in, ratio_gate], axis=1), "fs", axis=0, tiled=True),
+        [ratio_in.shape[1]],
+        axis=1,
+    )
     cols_in = factor_in
     cols_gate = factor_gate
     dir_in = jnp.dot(cols_in, piece_in, precision=lax.Precision.HIGHEST)

time: 570 us -> 522 us (0.916)
  waiting for transfers between devices: 442 us -> 393 us
    all_gather x2 -> x1, waiting for transfers between devices: 104 us -> 55.9 us  [local(): lax.all_gather(jnp.concatenate([ratio_in, ratio_gate], axis=1), 'fs', axi...]
  transfers between devices with their start and end apart: 7 -> 6, of which waited for: 7 -> 6; matrix products, arithmetic and copies ran while one was open for 8% -> 8% of each run, Pallas kernels for 0% -> 0%
where the time goes in v1:
time: 522 us
  waiting for transfers between devices  393 us (75%)
  matrix products  40.9 us (8%)
  blocking collectives  39.5 us (8%)
  local copies, waits for them, and re-layouts  24.3 us (5%)
  between operations  15.6 us (3%)
  other arithmetic  8.05 us (2%)
    all_gather x1, waiting for transfers between devices, local(): lax.all_gather(local_gate, 'fs', axis=0, tiled=True)  83.1 us
    reduce_scatter x1, waiting for transfers between devices, local(): lax.psum_scatter(jnp.concatenate([term_in, term_gate], axis=1), 'fs', sca...  80.4 us
    all_gather x1, waiting for transfers between devices, local(): lax.all_gather(local_in, 'fs', axis=0, tiled=True)  80 us
    all_gather x1, waiting for transfers between devices, local(): lax.all_gather(jnp.concatenate([ratio_in, ratio_gate], axis=1), 'fs', axi...  55.9 us
    all_gather x1, waiting for transfers between devices, local(): lax.all_gather(input_factor, 'fs', axis=0, tiled=True)  46.7 us
    all_gather x1, waiting for transfers between devices, local(): lax.all_gather(gate_factor, 'fs', axis=0, tiled=True)  45.5 us
    psum x1, blocking collectives, local(): lax.psum((jnp.sum(dir_in * dir_in), jnp.sum(dir_gate * dir_gate)), ('fs',...  39.5 us
    unnamed x25, local copies, waits for them, and re-layouts  24.3 us
  transfers between devices with their start and end apart: 6, of which 6 were waited for; matrix products, arithmetic and copies ran while one was open for 8% of the time, Pallas kernels for 0%

profile of v1, /device:TPU:0, one launch (start us, length us, event | category | flops | bytes accessed | tf_op | source)
XLA Modules:
  0.0 521.5 jit_solution(2477319089023916542)
XLA Ops:
  9.1 7.2 %fusion.8 = f32[2048,1024]{1,0:T(8,128)} fusion(bf16[768,2048]{1,0:T(8,128)(2,1)S(1)} %copy-done, bf16[768,1024]{1,0:T(8,128)(2,1)} %param.12), kind=kOutput, calls=%fused_computation.22 | convolution fusion | flops 3221225472 | bytes 13107200 | tf_op jit(solution)/shard_map/dot_general | solution.py:43
  16.2 5.7 %fusion.9 = f32[2048,1024]{1,0:T(8,128)} fusion(bf16[768,2048]{1,0:T(8,128)(2,1)S(1)} %copy-done, bf16[768,1024]{1,0:T(8,128)(2,1)S(1)} %copy-done.8), kind=kOutput, calls=%fused_computation.23 | convolution fusion | flops 3221225472 | bytes 13107200 | tf_op jit(solution)/shard_map/dot_general | solution.py:46
  21.9 46.7 %all-gather.6.cloned.1.call-done = bf16[2048,256]{1,0:T(8,128)(2,1)} async-done(((bf16[128,256]{1,0:T(8,128)(2,1)}), bf16[2048,256]{1,0:T(8,128)(2,1)}) %all-gather.6.cloned.1.call-update) | async-done | bytes 1048592 | tf_op jit(solution)/shard_map/all_gather | solution.py:40
  68.6 11.2 %convolution_bitcast_fusion.1 = f32[256,1024]{0,1:T(8,128)} fusion(f32[2048,1024]{1,0:T(8,128)} %fusion.8, bf16[2048,256]{1,0:T(8,128)(2,1)} %all-gather.6.cloned.1.call-done), kind=kOutput, calls=%fused_computation.2 | convolution fusion | flops 6442450944 | bytes 10485760 | tf_op jit(solution)/shard_map/dot_general | solution.py:51
  79.8 45.5 %all-gather.8.cloned.1.call-done = bf16[2048,256]{1,0:T(8,128)(2,1)} async-done(((bf16[128,256]{1,0:T(8,128)(2,1)}), bf16[2048,256]{1,0:T(8,128)(2,1)}) %all-gather.8.cloned.1.call-update) | async-done | bytes 1048592 | tf_op jit(solution)/shard_map/all_gather | solution.py:41
  125.3 9.5 %convolution_bitcast_fusion = f32[256,1024]{0,1:T(8,128)S(1)} fusion(f32[2048,1024]{1,0:T(8,128)} %fusion.9, bf16[2048,256]{1,0:T(8,128)(2,1)} %all-gather.8.cloned.1.call-done), kind=kOutput, calls=%fused_computation.1 | convolution fusion | flops 6442450944 | bytes 10485760 | tf_op jit(solution)/shard_map/dot_general | solution.py:52
  134.8 1.5 pad_maximum_fusion
  136.2 2.9 copy.65
  139.3 80.4 %reduce-scatter.4.cloned.1.call-done = f32[16,2048]{1,0:T(8,128)} async-done(((f32[256,2048]{1,0:T(8,128)}), f32[16,2048]{1,0:T(8,128)}) %reduce-scatter.4.cloned.1.call-update) | async-done | bytes 131088 | tf_op jit(solution)/shard_map/reduce_scatter | solution.py:53
  219.7 1.6 add_divide_fusion.1
  222.0 2.0 copy.59
  224.1 55.9 %all-gather.10.cloned.1.call-done = f32[256,2048]{1,0:T(8,128)} async-done(((f32[16,2048]{1,0:T(8,128)}), f32[256,2048]{1,0:T(8,128)}) %all-gather.10.cloned.1.call-update) | async-done | bytes 2097168 | tf_op jit(solution)/shard_map/all_gather | solution.py:61
  280.0 3.7 multiply_reduce_fusion
  283.7 3.6 multiply_reduce_fusion.1
  287.3 39.5 %all-reduce = (f32[]{:T(128)}, f32[]{:T(128)}) all-reduce(f32[]{:T(128)} %get-tuple-element.47, f32[]{:T(128)} %get-tuple-element.49), channel_id=1, replica_groups=mesh['fs'=16,'tp'=2] {'fs','tp'}, use_global_device_ids=true, to_apply=%region_2.0 | all-reduce | flops 2 | bytes 16 | tf_op jit(solution)/shard_map/psum | solution.py:69
  327.5 2.2 subtract_convert_fusion.1
  329.7 2.0 copy.60
  332.5 2.2 subtract_convert_fusion
  334.7 2.0 copy.61
  336.7 2.1 copy.62
  338.8 80.0 %all-gather.12.cloned.1.call-done = bf16[2048,1024]{0,1:T(8,128)(2,1)} async-done(((bf16[128,1024]{0,1:T(8,128)(2,1)}), bf16[2048,1024]{0,1:T(8,128)(2,1)}) %all-gather.12.cloned.1.call-update) | async-done | bytes 4194320 | tf_op jit(solution)/shard_map/all_gather | solution.py:77
  418.8 6.4 %copy.63 = bf16[2048,1024]{1,0:T(8,128)(2,1)} copy(bf16[2048,1024]{0,1:T(8,128)(2,1)} %all-gather.12.cloned.1.call-done) | data formatting | bytes 8388608
  425.2 83.1 %all-gather.14.cloned.1.call-done = bf16[2048,1024]{0,1:T(8,128)(2,1)} async-done(((bf16[128,1024]{0,1:T(8,128)(2,1)}), bf16[2048,1024]{0,1:T(8,128)(2,1)}) %all-gather.14.cloned.1.call-update) | async-done | bytes 4194320 | tf_op jit(solution)/shard_map/all_gather | solution.py:78
  508.3 6.4 %copy.64 = bf16[2048,1024]{1,0:T(8,128)(2,1)} copy(bf16[2048,1024]{0,1:T(8,128)(2,1)} %all-gather.14.cloned.1.call-done) | data formatting | bytes 8388608
  (31 shorter events, 2.7 us)
Async XLA Ops:
  7.2 1.9 copy-start
  7.2 61.4 %all-gather.6.cloned.1.call-start = ((), (), s32[]{:S(2)}) async-start(), calls=%async_computation.1 | async-start | bytes 1114112 | tf_op jit(solution)/shard_map/all_gather | solution.py:40
  7.9 117.4 %all-gather.8.cloned.1.call-start = ((), (), s32[]{:S(2)}) async-start(), calls=%async_computation.2 | async-start | bytes 1114112 | tf_op jit(solution)/shard_map/all_gather | solution.py:41
  8.7 211.0 %reduce-scatter.4.cloned.1.call-start = ((), (), s32[]{:S(2)}) async-start(), calls=%async_computation.6 | async-start | bytes 2228224 | tf_op jit(solution)/shard_map/reduce_scatter | solution.py:53
  9.1 7.2 %copy-start.8 = (bf16[768,1024]{1,0:T(8,128)(2,1)S(1)}, bf16[768,1024]{1,0:T(8,128)(2,1)}, u32[]{:S(2)}) copy-start(bf16[768,1024]{1,0:T(8,128)(2,1)} %param.13) | copy-start | bytes 4718596
  125.3 9.5 %copy-start.1 = (f32[256,1024]{0,1:T(8,128)S(1)}, f32[256,1024]{0,1:T(8,128)}, u32[]{:S(2)}) copy-start(f32[256,1024]{0,1:T(8,128)} %convolution_bitcast_fusion.1) | copy-start | bytes 3145732
  136.2 83.4 %copy-start.4 = (f32[16,1024]{1,0:T(8,128)S(1)}, f32[16,1024]{1,0:T(8,128)}, u32[]{:S(2)}) copy-start(f32[16,1024]{1,0:T(8,128)} %param.19) | copy-start | bytes 196612
  136.2 83.4 %copy-start.5 = (f32[16,1024]{1,0:T(8,128)S(1)}, f32[16,1024]{1,0:T(8,128)}, u32[]{:S(2)}) copy-start(f32[16,1024]{1,0:T(8,128)} %param.18) | copy-start | bytes 196612
  136.2 83.4 %copy-start.6 = (f32[16,1024]{1,0:T(8,128)S(1)}, f32[16,1024]{1,0:T(8,128)}, u32[]{:S(2)}) copy-start(f32[16,1024]{1,0:T(8,128)} %param.21) | copy-start | bytes 196612
  136.2 83.4 %copy-start.7 = (f32[16,1024]{1,0:T(8,128)S(1)}, f32[16,1024]{1,0:T(8,128)}, u32[]{:S(2)}) copy-start(f32[16,1024]{1,0:T(8,128)} %param.20) | copy-start | bytes 196612
  139.2 140.9 %copy-start.2 = (bf16[128,256]{1,0:T(8,128)(2,1)S(1)}, bf16[128,256]{1,0:T(8,128)(2,1)}, u32[]{:S(2)}) copy-start(bf16[128,256]{1,0:T(8,128)(2,1)} %param.17) | copy-start | bytes 196612
  139.2 144.5 %copy-start.3 = (bf16[128,256]{1,0:T(8,128)(2,1)S(1)}, bf16[128,256]{1,0:T(8,128)(2,1)}, u32[]{:S(2)}) copy-start(bf16[128,256]{1,0:T(8,128)(2,1)} %param.16) | copy-start | bytes 196612
  139.2 140.8 %all-gather.10.cloned.1.call-start = ((), (), s32[]{:S(2)}) async-start(), calls=%async_computation.3 | async-start | bytes 2228224 | tf_op jit(solution)/shard_map/all_gather | solution.py:61
  222.0 196.8 %all-gather.12.cloned.1.call-start = ((), (), s32[]{:S(2)}) async-start(), calls=%async_computation.4 | async-start | bytes 4456448 | tf_op jit(solution)/shard_map/all_gather | solution.py:77
  329.7 178.6 %all-gather.14.cloned.1.call-start = ((), (), s32[]{:S(2)}) async-start(), calls=%async_computation.5 | async-start | bytes 4456448 | tf_op jit(solution)/shard_map/all_gather | solution.py:78
Sparse Core Ops, SparseCore 0:
  10.7 57.7 all-gather.5
  71.3 53.9 all-gather.7
  139.3 80.3 reduce-scatter.3
  222.9 57.0 all-gather.9
  329.8 88.9 all-gather.11
  421.3 86.8 all-gather.13
